TPU v7x, 32 devices: a whole 2x2x4 slice. The times are simulated.
32 devices in a mesh: sp: 8 (over z, x), tp: 4 (over y, core).
Axes of the slice: x: 2, y: 2, z: 4, core: 2. Of those that a mesh axis runs over, the one named last changes fastest.
Arguments:
- tokens: bfloat16 [5120, 2048], P(('sp', 'tp')), may hold values from -44 to 44
- in_gain: float32 [2048], replicated, may hold values from 0.1 to 1.9
- w_x: bfloat16 [2048, 2048], P('sp', 'tp'), may hold values from -0.125 to 0.125
- w_z: bfloat16 [2048, 2048], P('sp', 'tp'), may hold values from -0.125 to 0.125
- w_b: bfloat16 [2048, 1024], P('sp', 'tp'), may hold values from -0.125 to 0.125
- w_c: bfloat16 [2048, 1024], P('sp', 'tp'), may hold values from -0.125 to 0.125
- w_dt: bfloat16 [2048, 32], replicated, may hold values from -0.125 to 0.125
- conv_x: float32 [4, 2048], replicated, may hold values from -3 to 3
- conv_b: float32 [4, 1024], replicated, may hold values from -3 to 3
- conv_c: float32 [4, 1024], replicated, may hold values from -3 to 3
- dt_bias: float32 [32], replicated, may hold values from -15 to -3.5
- a_log: float32 [32], replicated, may hold values from -0.5 to 0.5
- out_gain: float32 [2048], replicated, may hold values from 0.1 to 1.9
- w_out: bfloat16 [2048, 2048], P('tp', 'sp'), may hold values from -0.125 to 0.125
Outputs:
- mixer_out: bfloat16 [5120, 2048], P(('sp', 'tp'))
All inputs are finite; a program needn't handle non-finite values.
Results may differ from a plain program's by a relative error of at most 0.015.
Values may be sent and summed in bfloat16 or wider, within the bound.
A program may use at most 128 MiB of HBM per device.

v0:
```python
import jax
import jax.numpy as jnp
from jax import lax
from jax.sharding import PartitionSpec as P

HEAD_DIM = 64
STATE = 128
CONV = 4
BLOCK = 128


EPS = 1e-06
HIGH = lax.Precision.HIGHEST


def carried_in(part, axis, combine, identity):
    place = lax.axis_index(axis)
    gathered = jax.tree.map(lambda a: lax.all_gather(a, axis), part)
    state = jax.tree.map(lambda a, e: jnp.zeros_like(a) + jnp.asarray(e, a.dtype), part, identity)

    def one(lap, state):
        return combine(
            state, jax.tree.map(lambda a: lax.dynamic_index_in_dim(a, lap, 0, False), gathered)
        )

    return lax.fori_loop(0, place, one, state)


def from_behind(value, axis, steps):
    count = lax.axis_size(axis)
    first, last = (max(0, -steps), min(count, count - steps))
    return lax.ppermute(value, axis, [(source, source + steps) for source in range(first, last)])


def inverse_rms(values):
    return lax.rsqrt(jnp.mean(values * values, axis=-1, keepdims=True) + EPS)


def causal_conv(prev_rows, new_rows, kernel):
    joined = jnp.concatenate([prev_rows, new_rows], axis=0).astype(jnp.float32)
    row_count = new_rows.shape[0]
    summed = jnp.zeros(new_rows.shape, jnp.float32)
    for offset in range(kernel.shape[0]):
        summed = summed + kernel[offset] * joined[offset : offset + row_count]
    return jax.nn.silu(summed)


def fold_single(gathered):

    def fold_step(total_part, rows_part, first_row):
        return jnp.dot(gathered, rows_part, preferred_element_type=jnp.float32)

    return fold_step


def fold_products(gathered, totals, weight_rows, first_row):
    single = fold_single(gathered)
    return tuple(
        (
            single(total_part, rows_part, first_row)
            for total_part, rows_part in zip(totals, weight_rows)
        )
    )


def inner_part(cum_decay, b_rows, c_rows, scaled_x, causal):
    scores = jnp.einsum("blgn,bsgn->bgls", c_rows, b_rows, precision=HIGH)
    decay_gap = cum_decay[:, :, None] - cum_decay[:, None, :]
    causal_mask = causal[None, :, :, None, None]
    within = jnp.where(causal_mask, jnp.exp(jnp.where(causal_mask, decay_gap, 0.0)), 0.0)
    return jnp.einsum("bgls,blsgh,bsghp->blghp", scores, within, scaled_x, precision=HIGH)


def carried_part(c_rows, states, cum_decay):
    return jnp.einsum("blgn,bghpn,blgh->blghp", c_rows, states, jnp.exp(cum_decay), precision=HIGH)


def run_blocks(block_states, block_decay, start_state):

    def advance(run_state, inputs):
        fresh_state, factor = inputs
        return (run_state * factor[:, :, None, None] + fresh_state, run_state)

    final_state, entering = lax.scan(advance, start_state, (block_states, block_decay))
    return (entering, final_state)


def chain(earlier, later):
    return (earlier[0] * later[0], earlier[1] * later[0][:, :, None, None] + later[1])


def carry_in(total_decay, final_state):
    identity = (jnp.ones_like(total_decay), jnp.zeros_like(final_state))
    before = carried_in((total_decay, final_state), "sp", chain, identity)
    return before[1]


def body(
    tokens,
    in_gain,
    w_x,
    w_z,
    w_b,
    w_c,
    w_dt,
    conv_x,
    conv_b,
    conv_c,
    dt_bias,
    a_log,
    out_gain,
    w_out,
):
    share_index = lax.axis_index("tp")
    width_x = w_x.shape[1]
    width_b = w_b.shape[1]
    heads_here = width_x // HEAD_DIM
    groups_here = width_b // STATE
    group_heads = heads_here // groups_here
    kernel_x = lax.dynamic_slice_in_dim(conv_x, share_index * width_x, width_x, 1)
    kernel_b = lax.dynamic_slice_in_dim(conv_b, share_index * width_b, width_b, 1)
    kernel_c = lax.dynamic_slice_in_dim(conv_c, share_index * width_b, width_b, 1)
    bias_here = lax.dynamic_slice_in_dim(dt_bias, share_index * heads_here, heads_here, 0)
    rate_here = jnp.exp(lax.dynamic_slice_in_dim(a_log, share_index * heads_here, heads_here, 0))
    gain_here = lax.dynamic_slice_in_dim(out_gain, share_index * width_x, width_x, 0)
    dt_weight = lax.dynamic_slice_in_dim(w_dt, share_index * heads_here, heads_here, 1)
    values = tokens.astype(jnp.float32)
    normed = (values * inverse_rms(values) * in_gain).astype(jnp.bfloat16)
    gathered = lax.all_gather(normed, "tp", axis=0, tiled=True)
    seg_rows = gathered.shape[0]
    blocks = seg_rows // BLOCK
    empty_x = jnp.zeros((seg_rows, width_x), jnp.float32)
    empty_b = jnp.zeros((seg_rows, width_b), jnp.float32)
    projected = fold_products(
        gathered,
        (empty_x, empty_x, empty_b, empty_b),
        (
            lax.all_gather(w_x, "sp", axis=0, tiled=True),
            lax.all_gather(w_z, "sp", axis=0, tiled=True),
            lax.all_gather(w_b, "sp", axis=0, tiled=True),
            lax.all_gather(w_c, "sp", axis=0, tiled=True),
        ),
        jnp.int32(0),
    )
    proj_x, gate_rows, proj_b, proj_c = [
        summed_part.astype(jnp.bfloat16) for summed_part in projected
    ]
    dt_raw = jnp.dot(gathered, dt_weight, preferred_element_type=jnp.float32)
    conv_keep = CONV - 1
    tail_start = seg_rows - conv_keep
    prev_x, prev_b, prev_c = from_behind(
        (proj_x[tail_start:], proj_b[tail_start:], proj_c[tail_start:]), "sp", 1
    )
    conv_xs = causal_conv(prev_x, proj_x, kernel_x)
    conv_bs = causal_conv(prev_b, proj_b, kernel_b)
    conv_cs = causal_conv(prev_c, proj_c, kernel_c)
    step_size = jax.nn.softplus(dt_raw + bias_here)
    log_decay = (-step_size * rate_here).reshape(blocks, BLOCK, groups_here, group_heads)
    causal = lax.broadcasted_iota(jnp.int32, (BLOCK, BLOCK), 0) >= lax.broadcasted_iota(
        jnp.int32, (BLOCK, BLOCK), 1
    )
    cum_decay = jnp.einsum("ls,bsgh->blgh", causal.astype(jnp.float32), log_decay, precision=HIGH)
    scaled_x = (conv_xs.reshape(seg_rows, heads_here, HEAD_DIM) * step_size[:, :, None]).reshape(
        blocks, BLOCK, groups_here, group_heads, HEAD_DIM
    )
    b_rows = conv_bs.reshape(blocks, BLOCK, groups_here, STATE)
    c_rows = conv_cs.reshape(blocks, BLOCK, groups_here, STATE)
    block_total = cum_decay[:, BLOCK - 1]
    tail_weight = jnp.exp(block_total[:, None] - cum_decay)
    block_states = jnp.einsum(
        "blgn,blgh,blghp->bghpn", b_rows, tail_weight, scaled_x, precision=HIGH
    )
    block_decay = jnp.exp(block_total)
    total_decay = jnp.exp(jnp.sum(block_total, axis=0))
    start_state = jnp.zeros(block_states.shape[1:], jnp.float32)
    entering, final_state = run_blocks(block_states, block_decay, start_state)
    incoming = carry_in(total_decay, final_state)

    def per_block(run_state, inputs):
        cum_here, b_here, c_here, x_here, fresh_state, factor = inputs
        output = inner_part(cum_here[None], b_here[None], c_here[None], x_here[None], causal)[0]
        output = output + carried_part(c_here[None], run_state[None], cum_here[None])[0]
        return (run_state * factor[:, :, None, None] + fresh_state, output)

    unused, heads_out = lax.scan(
        per_block, incoming, (cum_decay, b_rows, c_rows, scaled_x, block_states, block_decay)
    )
    gated_out = heads_out.reshape(seg_rows, width_x) * jax.nn.silu(gate_rows.astype(jnp.float32))
    grouped = gated_out.reshape(seg_rows, groups_here, width_x // groups_here)
    mixed_rows = ((grouped * inverse_rms(grouped)).reshape(seg_rows, width_x) * gain_here).astype(
        jnp.bfloat16
    )
    partial_sum = jnp.dot(
        mixed_rows,
        lax.all_gather(w_out, "sp", axis=1, tiled=True),
        preferred_element_type=jnp.float32,
    )
    return lax.psum_scatter(partial_sum.astype(jnp.bfloat16), "tp", scatter_dimension=0, tiled=True)


def solution(mesh):
    in_specs = (
        P(("sp", "tp"), None),
        P(),
        P("sp", "tp"),
        P("sp", "tp"),
        P("sp", "tp"),
        P("sp", "tp"),
        P(),
        P(),
        P(),
        P(),
        P(),
        P(),
        P(),
        P("tp", "sp"),
    )
    out_specs = P(("sp", "tp"), None)
    return jax.shard_map(body, mesh=mesh, in_specs=in_specs, out_specs=out_specs, check_vma=False)
```

profile of v0, /device:TPU:24, one launch (start us, length us, event | category | flops | bytes accessed | tf_op | source)
XLA Modules:
  0.0 364.8 jit_solution(4335275581894576468)
XLA Ops:
  6.5 1.3 fusion.22
  7.9 2.1 fusion.24
  10.1 0.7 all-gather.15.cloned.1.call-update
  10.9 0.7 all-gather.13.cloned.1.call-update
  11.6 0.5 all-gather.17.cloned.1.call-update
  12.4 1.5 constant_dynamic-slice_fusion.5
  13.9 0.9 constant_dynamic-slice_fusion.6
  14.8 21.9 %all-gather.11.cloned.1.call-done = bf16[640,2048]{1,0:T(8,128)(2,1)} async-done(((bf16[160,2048]{1,0:T(8,128)(2,1)}), bf16[640,2048]{1,0:T(8,128)(2,1)}) %all-gather.11.cloned.1.call-update) | async-done | bytes 2621456 | tf_op jit(solution)/shard_map/all_gather | solution.py:129
  36.7 2.7 negate_multiply_fusion
  39.6 0.7 slice_reduce_fusion
  40.4 37.5 %all-gather.15.cloned.1.call-done = bf16[2048,256]{1,0:T(8,128)(2,1)} async-done(((bf16[256,256]{1,0:T(8,128)(2,1)}), bf16[2048,256]{1,0:T(8,128)(2,1)}) %all-gather.15.cloned.1.call-update) | async-done | bytes 1048592 | tf_op jit(solution)/shard_map/all_gather | solution.py:140
  77.9 2.1 convolution_convert_fusion.4
  80.0 2.5 collective-permute-start.1
  82.4 45.2 %all-gather.13.cloned.1.call-done = bf16[2048,512]{1,0:T(8,128)(2,1)} async-done(((bf16[256,512]{1,0:T(8,128)(2,1)}), bf16[2048,512]{1,0:T(8,128)(2,1)}) %all-gather.13.cloned.1.call-update) | async-done | bytes 2097168 | tf_op jit(solution)/shard_map/all_gather | solution.py:138
  127.7 3.1 convolution_convert_fusion.2
  130.9 0.7 copy-done.3
  131.6 2.5 collective-permute-start
  134.1 0.6 copy.69
  135.6 2.4 collective-permute-done
  138.2 0.8 divide_multiply_fusion
  139.0 1.5 copy.68
  140.5 1.4 reshape.103
  141.9 1.7 broadcast_multiply_fusion.1
  143.6 1.4 fusion.32
  145.0 0.7 while.39
  145.7 0.7 copy-done.1
  147.0 0.7 all-gather.21.cloned.1.call-update
  147.8 0.9 constant_dynamic-slice_fusion.7
  148.7 0.8 dynamic_slice.66
  149.5 19.2 %all-gather.17.cloned.1.call-done = bf16[2048,256]{1,0:T(8,128)(2,1)} async-done(((bf16[256,256]{1,0:T(8,128)(2,1)}), bf16[2048,256]{1,0:T(8,128)(2,1)}) %all-gather.17.cloned.1.call-update) | async-done | bytes 1048592 | tf_op jit(solution)/shard_map/all_gather | solution.py:141
  168.7 2.9 convolution_convert_fusion.3
  171.6 2.5 collective-permute-start.2
  174.1 15.2 %all-gather.2 = f32[8,2,4]{2,1,0:T(2,128)S(1)} all-gather(f32[1,2,4]{2,1,0:T(2,128)S(1)} %exponential_bitcast_fusion.1), channel_id=2, replica_groups=mesh['sp'=8,'tp'=4] {'sp'}, dimensions={0}, use_global_device_ids=true | all-gather | bytes 288 | tf_op jit(solution)/shard_map/all_gather | solution.py:18
  189.3 1.2 divide_multiply_fusion.1
  190.6 1.4 reshape.105
  192.0 26.3 %all-gather.23.cloned.1.call-done = f32[16,4,64,128]{3,2,1,0:T(8,128)} async-done(((f32[2,4,64,128]{3,2,1,0:T(8,128)}), f32[16,4,64,128]{3,2,1,0:T(8,128)}) %all-gather.23.cloned.1.call-update) | async-done | bytes 2097168 | tf_op jit(solution)/shard_map/all_gather | solution.py:18
  218.4 6.8 %while.37 = (s32[]{:T(128)}, f32[2,4,64,128]{3,2,1,0:T(8,128)S(1)}, s32[]{:T(128)}, f32[8,2,4]{2,1,0:T(2,128)S(1)}, f32[8,2,4,64,128]{4,3,2,1,0:T(8,128)}, /*index=5*/s32[]{:T(128)}, s32[]{:T(128)}, s32[]{:T(128)}) while((s32[]{:T(128)}, f32[2,4,64,128]{3,2,1,0:T(8,128)S(1)}, s32[]{:T(128)}, f32[8,2,4]{2,1,0:T(2,128)S(1)}, ...), condition=%wide.region_5.6_spmd, body=%wide.region_4.5_spmd.sunk | while | flops 131077 | bytes 786655 | solution.py:26
  218.4 1.1 bitcast_add_fusion.6
  219.5 1.1 bitcast_add_fusion.6
  220.6 1.1 bitcast_add_fusion.6
  221.7 1.1 bitcast_add_fusion.6
  222.8 1.1 bitcast_add_fusion.6
  223.9 1.1 bitcast_add_fusion.6
  225.2 24.1 %while.38 = (s32[]{:T(128)}, f32[2,4,64,128]{3,2,1,0:T(8,128)S(1)}, f32[5,128,2,4,64]{1,4,3,2,0:T(8,128)}, f32[5,2,4]{2,1,0:T(2,128)S(1)}, f32[5,2,4,64,128]{4,3...) while((s32[]{:T(128)}, f32[2,4,64,128]{3,2,1,0:T(8,128)S(1)}, ...), condition=%wide.region_7.8_spmd.clone.clone, body=%wide.region_6.7_spmd.clone.clone.sunk | while | flops 252461056 | bytes 3863257 | solution.py:185
  226.1 1.9 constant_dynamic-slice_fusion.13
  227.9 1.9 fusion.77
  230.9 1.9 constant_dynamic-slice_fusion.13
  232.8 1.9 fusion.77
  235.7 1.9 constant_dynamic-slice_fusion.13
  237.6 1.9 fusion.77
  240.5 1.9 constant_dynamic-slice_fusion.13
  242.4 1.9 fusion.77
  245.3 1.9 constant_dynamic-slice_fusion.13
  247.2 2.0 fusion.77
  249.3 3.0 copy.89
  252.3 2.8 reshape.123
  255.1 13.0 %all-gather.19.cloned.1.call-done = bf16[2048,512]{1,0:T(8,128)(2,1)} async-done(((bf16[256,512]{1,0:T(8,128)(2,1)}), bf16[2048,512]{1,0:T(8,128)(2,1)}) %all-gather.19.cloned.1.call-update) | async-done | bytes 2097168 | tf_op jit(solution)/shard_map/all_gather | solution.py:139
  268.1 5.5 %fusion.49 = (f32[640,512]{1,0:T(8,128)S(1)}, f32[640,512]{1,0:T(8,128)}) fusion(f32[640,512]{1,0:T(8,128)} %reshape.123, bf16[640,2048]{1,0:T(8,128)(2,1)} %all-gather.11.cloned.1.call-done, bf16[2048,512]{1,0:T(8,128)(2,1)} %all-gather.19.cloned.1.call-done), kind=kOutput, calls=%fused_computation.107 | convolution fusion | flops 1344798720 | bytes 8650752 | tf_op jit(solution)/shard_map/dot_general | solution.py:51
  273.6 0.8 mul.303
  274.5 0.7 reduce_sum.29
  275.3 0.8 mul.304
  276.3 42.4 %all-gather.21.cloned.1.call-done = bf16[512,2048]{1,0:T(8,128)(2,1)} async-done(((bf16[512,256]{1,0:T(8,128)(2,1)}), bf16[512,2048]{1,0:T(8,128)(2,1)}) %all-gather.21.cloned.1.call-update) | async-done | bytes 2097168 | tf_op jit(solution)/shard_map/all_gather | solution.py:195
  318.6 4.6 %convolution_convert_fusion = bf16[640,2048]{1,0:T(8,128)(2,1)} fusion(bf16[512,2048]{1,0:T(8,128)(2,1)} %all-gather.21.cloned.1.call-done, f32[640,512]{1,0:T(8,128)S(1)} %copy-done.11, f32[640,512]{1,0:T(8,128)S(1)} %bitcast.131, f32[512]{0:T(512)S(1)} %dynamic_slice.66), kind=kOutput, calls=%fused_computation.38 | convolution fusion | flops 1344471040 | bytes 7342080 | tf_op jit(solution)/shard_map/dot_general | solution.py:193
  323.3 34.7 %reduce-scatter.2.cloned.1.call-done = bf16[160,2048]{1,0:T(8,128)(2,1)} async-done(((bf16[640,2048]{1,0:T(8,128)(2,1)}), bf16[160,2048]{1,0:T(8,128)(2,1)}) %reduce-scatter.2.cloned.1.call-update) | async-done | bytes 655376 | tf_op jit(solution)/shard_map/reduce_scatter | solution.py:198
  (113 shorter events, 8.0 us)
Async XLA Ops:
  6.5 30.2 %copy-start = (bf16[2048,32]{0,1:T(8,128)(2,1)S(1)}, bf16[2048,32]{0,1:T(8,128)(2,1)}, u32[]{:S(2)}) copy-start(bf16[2048,32]{0,1:T(8,128)(2,1)} %param.26) | copy-start | bytes 393220
  6.5 30.2 %all-gather.11.cloned.1.call-start = ((), (), s32[]{:S(2)}) async-start(), calls=%async_computation.1 | async-start | bytes 3276800 | tf_op jit(solution)/shard_map/all_gather | solution.py:129
  7.9 4.3 %copy-start.9 = (f32[32]{0:T(128)S(1)}, f32[32]{0:T(128)}, u32[]{:S(2)}) copy-start(f32[32]{0:T(128)} %param.31) | copy-start | bytes 388
  7.9 4.4 %copy-start.10 = (f32[32]{0:T(128)S(1)}, f32[32]{0:T(128)}, u32[]{:S(2)}) copy-start(f32[32]{0:T(128)} %param.30) | copy-start | bytes 388
  10.1 67.8 %all-gather.15.cloned.1.call-start = ((), (), s32[]{:S(2)}) async-start(), calls=%async_computation.3 | async-start | bytes 1179648 | tf_op jit(solution)/shard_map/all_gather | solution.py:140
  10.8 116.8 %all-gather.13.cloned.1.call-start = ((), (), s32[]{:S(2)}) async-start(), calls=%async_computation.2 | async-start | bytes 2359296 | tf_op jit(solution)/shard_map/all_gather | solution.py:138
  11.6 157.1 %all-gather.17.cloned.1.call-start = ((), (), s32[]{:S(2)}) async-start(), calls=%async_computation.4 | async-start | bytes 1179648 | tf_op jit(solution)/shard_map/all_gather | solution.py:141
  12.1 206.2 %all-gather.23.cloned.1.call-start = ((), (), s32[]{:S(2)}) async-start(), calls=%async_computation.8 | async-start | bytes 2359296 | tf_op jit(solution)/shard_map/all_gather | solution.py:18
  36.7 41.1 %copy-start.2 = (bf16[640,2048]{1,0:T(8,128)(2,1)S(1)}, bf16[640,2048]{1,0:T(8,128)(2,1)}, u32[]{:S(2)}) copy-start(bf16[640,2048]{1,0:T(8,128)(2,1)} %all-gather.11.cloned.1.call-done) | copy-start | bytes 7864324
  80.0 54.8 %collective-permute-start.1 = (bf16[3,256]{1,0:T(4,128)(2,1)S(1)}, bf16[3,256]{1,0:T(4,128)(2,1)S(1)}, u32[]{:S(2)}, u32[]{:S(2)}) collective-permute-start(bf16[3,256]{1,0:T(4,128)(2,1)S(1)} %slice.118), channel_id=1, source_target_pairs={{0,4},{4,8},{8,12},{12,16},{16,20},{20,24},{24,28},{1,5},{5,9},{9,... | collective-permute-start | bytes 4616 | tf_op jit(solution)/shard_map/ppermute | solution.py:32
  130.8 0.8 copy-start.3
  131.6 6.4 %collective-permute-start = (bf16[3,512]{1,0:T(4,128)(2,1)S(1)}, bf16[3,512]{1,0:T(4,128)(2,1)S(1)}, u32[]{:S(2)}, u32[]{:S(2)}) collective-permute-start(bf16[3,512]{1,0:T(4,128)(2,1)S(1)} %slice.113), channel_id=1, source_target_pairs={{0,4},{4,8},{8,12},{12,16},{16,20},{20,24},{24,28},{1,5},{5,9},{9,... | collective-permute-start | bytes 9224 | tf_op jit(solution)/shard_map/ppermute | solution.py:32
  135.3 2.7 copy-start.4
  135.6 2.6 copy-start.6
  135.6 2.6 copy-start.7
  140.5 1.4 copy-start.5
  145.7 0.7 copy-start.1
  146.4 121.7 %all-gather.19.cloned.1.call-start = ((), (), s32[]{:S(2)}) async-start(), calls=%async_computation.5 | async-start | bytes 2359296 | tf_op jit(solution)/shard_map/all_gather | solution.py:139
  147.0 171.6 %all-gather.21.cloned.1.call-start = ((), (), s32[]{:S(2)}) async-start(), calls=%async_computation.6 | async-start | bytes 2359296 | tf_op jit(solution)/shard_map/all_gather | solution.py:195
  147.8 210.3 %reduce-scatter.2.cloned.1.call-start = ((), (), s32[]{:S(2)}) async-start(), calls=%async_computation.7 | async-start | bytes 3276800 | tf_op jit(solution)/shard_map/reduce_scatter | solution.py:198
  149.5 24.6 %copy-start.8 = (f32[2,4]{1,0:T(2,128)S(1)}, f32[2,4]{1,0:T(2,128)}, u32[]{:S(2)}) copy-start(f32[2,4]{1,0:T(2,128)} %get-tuple-element.254) | copy-start | bytes 100
  171.6 17.7 %collective-permute-start.2 = (bf16[3,256]{1,0:T(4,128)(2,1)S(1)}, bf16[3,256]{1,0:T(4,128)(2,1)S(1)}, u32[]{:S(2)}, u32[]{:S(2)}) collective-permute-start(bf16[3,256]{1,0:T(4,128)(2,1)S(1)} %slice.123), channel_id=1, source_target_pairs={{0,4},{4,8},{8,12},{12,16},{16,20},{20,24},{24,28},{1,5},{5,9},{9,... | collective-permute-start | bytes 4616 | tf_op jit(solution)/shard_map/ppermute | solution.py:32
  276.1 42.5 %copy-start.11 = (f32[640,512]{1,0:T(8,128)S(1)}, f32[640,512]{1,0:T(8,128)}, u32[]{:S(2)}) copy-start(f32[640,512]{1,0:T(8,128)} %get-tuple-element.310) | copy-start | bytes 3932164
Sparse Core Ops, SparseCore 0:
  10.2 26.4 all-gather.10
  38.9 38.9 all-gather.14
  80.0 47.6 all-gather.12
  129.6 39.0 all-gather.16
  170.7 47.6 all-gather.22
  220.3 47.7 all-gather.18
  270.1 48.4 all-gather.20
  323.4 34.5 reduce-scatter.1
where the time goes:
time: 368 us; the launch traced here: 365 us
  waiting for transfers between devices  246 us (67%)
  matrix products  36 us (10%)
  local copies, waits for them, and re-layouts  28.3 us (8%)
  other arithmetic  17 us (5%)
  blocking collectives  15.2 us (4%)
  between operations  13.9 us (4%)
  starting transfers between devices  7.66 us (2%)
    all_gather x1, waiting for transfers between devices, body(): lax.all_gather(w_x, 'sp', axis=0, tiled=True)  45.2 us
    all_gather x1, waiting for transfers between devices, body(): lax.all_gather(w_out, 'sp', axis=1, tiled=True)  42.4 us
    all_gather x1, waiting for transfers between devices, body(): lax.all_gather(w_b, 'sp', axis=0, tiled=True)  37.5 us
    reduce_scatter x1, waiting for transfers between devices, body(): lax.psum_scatter(partial_sum.astype(jnp.bfloat16), 'tp', scatter_dimensio...  34.7 us
    all_gather x1, waiting for transfers between devices, carried_in(): gathered = jax.tree.map(lambda a: lax.all_gather(a, axis), part)  26.3 us
    all_gather x1, waiting for transfers between devices, body(): gathered = lax.all_gather(normed, 'tp', axis=0, tiled=True)  21.9 us
    all_gather x1, waiting for transfers between devices, body(): lax.all_gather(w_c, 'sp', axis=0, tiled=True)  19.2 us
    all_gather x1, blocking collectives, carried_in(): gathered = jax.tree.map(lambda a: lax.all_gather(a, axis), part)  15.2 us
  transfers between devices with their start and end apart: 11, of which 9 were waited for; matrix products, arithmetic and copies ran while one was open for 20% of the time, Pallas kernels for 0%

commit v1 on v0

--- a/solution.py
+++ b/solution.py
@@ -1,6 +1,8 @@
 import jax
 import jax.numpy as jnp
 from jax import lax
+from jax.experimental import pallas as pl
+from jax.experimental.pallas import tpu as pltpu
 from jax.sharding import PartitionSpec as P
 
 HEAD_DIM = 64
@@ -198,6 +200,458 @@
     return lax.psum_scatter(partial_sum.astype(jnp.bfloat16), "tp", scatter_dimension=0, tiled=True)
 
 
+MESH = pl.DeviceIdType.MESH
+BF16 = jnp.bfloat16
+F32 = jnp.float32
+HALO = 16
+
+
+def mixer_kernel(
+    n_sp,
+    n_tp,
+    tok_ref,
+    in_gain_ref,
+    w_x_ref,
+    w_bc_ref,
+    w_z_ref,
+    w_o_ref,
+    w_dt_ref,
+    taps_x_ref,
+    taps_bc_ref,
+    bias_ref,
+    rate_ref,
+    gain_ref,
+    out_ref,
+    nall,
+    gath,
+    gath_o,
+    proj,
+    scaled,
+    bc_rows,
+    log_step,
+    cum_seg,
+    heads_cum,
+    entering,
+    state,
+    y_buf,
+    mixed,
+    part,
+    pair_in,
+    slot_f,
+    slot_a,
+    tok_send,
+    tok_recv,
+    halo_send,
+    halo_recv,
+    z_send,
+    x_send,
+    w_recv,
+    own_sem,
+    st_send,
+    st_recv,
+    rs_send,
+    rs_recv,
+):
+    sp = lax.axis_index("sp")
+    tp = lax.axis_index("tp")
+    share = tok_ref.shape[0]
+    seg_rows = share * n_tp
+    blocks = seg_rows // BLOCK
+    width = w_x_ref.shape[1]
+    half = width // 2
+    heads_here = width // HEAD_DIM
+    groups_here = half // STATE
+    group_heads = heads_here // groups_here
+    group_width = width // groups_here
+    depth = w_x_ref.shape[0]
+    n_z = n_sp // 2
+    beside = sp + 1 - 2 * lax.rem(sp, 2)
+    own_refs = (w_x_ref, w_bc_ref, w_z_ref, w_o_ref)
+
+    def remote(src, dst, send, recv, where):
+        return pltpu.make_async_remote_copy(
+            src_ref=src, dst_ref=dst, send_sem=send, recv_sem=recv, device_id=where,
+            device_id_type=MESH,
+        )
+
+    def place(chunk, source):
+        if chunk == 3:
+            cols = w_o_ref.shape[1]
+            return gath_o.at[:, pl.ds(pl.multiple_of(source * cols, cols), cols)]
+        return gath.at[chunk, pl.ds(pl.multiple_of(source * depth, depth), depth), :]
+
+    values = tok_ref[...].astype(F32)
+    normed = (values * inverse_rms(values) * in_gain_ref[...]).astype(BF16)
+
+    def token_rows(index):
+        return nall.at[pl.ds(pl.multiple_of(HALO + index * share, 16), share), :]
+
+    token_rows(tp)[...] = normed
+
+    def token_copy(step):
+        return remote(
+            token_rows(tp), token_rows(tp), tok_send.at[step - 1], tok_recv.at[tp],
+            (sp, lax.rem(tp + step, n_tp)),
+        )
+
+    def halo_copy(target):
+        return remote(
+            nall.at[pl.ds(seg_rows, HALO), :], nall.at[pl.ds(0, HALO), :], halo_send.at[target],
+            halo_recv.at[0], (lax.rem(sp + 1, n_sp), target),
+        )
+
+    @pl.when(tp == n_tp - 1)
+    def _():
+        for target in range(n_tp):
+            halo_copy(target).start()
+
+    def z_copy(chunk, step):
+        return remote(
+            own_refs[chunk], place(chunk, sp), z_send.at[chunk, step], w_recv.at[chunk, sp],
+            (lax.rem(sp + 2 * step, n_sp), tp),
+        )
+
+    def x_copy(chunk, step):
+        source = lax.rem(sp + n_sp - 2 * step, n_sp)
+        src = own_refs[chunk] if step == 0 else place(chunk, source)
+        return remote(
+            src, place(chunk, source), x_send.at[chunk, step], w_recv.at[chunk, source],
+            (beside, tp),
+        )
+
+    def arrival(chunk, source):
+        return remote(
+            own_refs[chunk], place(chunk, source), z_send.at[chunk, 0], w_recv.at[chunk, source],
+            (beside, tp),
+        )
+
+    def own_copy(chunk):
+        return pltpu.make_async_copy(own_refs[chunk], place(chunk, sp), own_sem.at[chunk])
+
+    for chunk in range(4):
+        x_copy(chunk, 0).start()
+        for step in range(1, n_z):
+            z_copy(chunk, step).start()
+        if chunk == 0:
+            for step in range(1, n_tp):
+                token_copy(step).start()
+        own_copy(chunk).start()
+
+    def forward(chunk):
+        for step in range(1, n_z):
+            source = lax.rem(sp + n_sp - 2 * step, n_sp)
+            arrival(chunk, source).wait_recv()
+            x_copy(chunk, step).start()
+
+    def finish(chunk):
+        own_copy(chunk).wait()
+        for step in range(n_z):
+            arrival(chunk, lax.rem(beside + n_sp - 2 * step, n_sp)).wait_recv()
+
+    forward(0)
+    for step in range(1, n_tp):
+        source = lax.rem(tp + n_tp - step, n_tp)
+        remote(
+            token_rows(source), token_rows(source), tok_send.at[0], tok_recv.at[source],
+            (sp, source),
+        ).wait_recv()
+    halo_copy(0).wait_recv()
+
+    @pl.when(tp == n_tp - 1)
+    def _():
+        for target in range(n_tp):
+            halo_copy(target).wait_send()
+
+    for step in range(1, n_tp):
+        token_copy(step).wait_send()
+
+    @pl.when(sp == 0)
+    def _():
+        nall[pl.ds(0, HALO), :] = jnp.zeros((HALO, nall.shape[1]), BF16)
+
+    raw = jnp.dot(nall[pl.ds(HALO, seg_rows), :], w_dt_ref[...], preferred_element_type=F32)
+    raw = raw + bias_ref[...]
+    log_step[...] = jnp.maximum(raw, 0.0) + jnp.log1p(jnp.exp(-jnp.abs(raw)))
+    lanes = log_step.shape[1]
+    spread = (
+        lax.broadcasted_iota(jnp.int32, (lanes, width), 0)
+        == lax.broadcasted_iota(jnp.int32, (lanes, width), 1) // HEAD_DIM
+    ).astype(F32)
+    causal = lax.broadcasted_iota(jnp.int32, (BLOCK, BLOCK), 0) >= lax.broadcasted_iota(
+        jnp.int32, (BLOCK, BLOCK), 1
+    )
+
+    def project(chunk):
+        proj[...] = (
+            jnp.dot(nall[...], gath[chunk], preferred_element_type=F32).astype(BF16).astype(F32)
+        )
+
+    def conv(block, taps):
+        summed = jnp.zeros((BLOCK, width), F32)
+        start = block * BLOCK + HALO - (CONV - 1)
+        for offset in range(CONV):
+            summed = summed + taps[offset : offset + 1, :] * proj[
+                start + offset : start + offset + BLOCK, :
+            ]
+        return summed / (1.0 + jnp.exp(-summed))
+
+    forward(1)
+    finish(0)
+    project(0)
+    for block in range(blocks):
+        rows = pl.ds(block * BLOCK, BLOCK)
+        step_here = jnp.dot(log_step[rows, :], spread, precision=HIGH, preferred_element_type=F32)
+        scaled[rows, :] = conv(block, taps_x_ref[...]) * step_here
+
+    finish(1)
+    project(1)
+    for block in range(blocks):
+        rows = pl.ds(block * BLOCK, BLOCK)
+        bc_rows[rows, :] = conv(block, taps_bc_ref[...]).astype(BF16)
+
+    def rows_of(block):
+        return pl.ds(pl.multiple_of(block * BLOCK, BLOCK), BLOCK)
+
+    state[...] = jnp.zeros_like(state)
+    tri = causal.astype(F32)
+
+    def states_of(block, total):
+        rows = rows_of(block)
+        log_rate = -log_step[rows, :] * rate_ref[...]
+        cum = jnp.dot(tri, log_rate, precision=HIGH, preferred_element_type=F32)
+        heads_cum[rows, :] = cum
+        wide = jnp.dot(cum, spread, precision=HIGH, preferred_element_type=F32)
+        cum_seg[rows, :] = wide
+        last = wide[BLOCK - 1 : BLOCK, :]
+        weighted = (scaled[rows, :] * jnp.exp(last - wide)).astype(BF16)
+        old = state[...]
+        entering[block] = old.astype(BF16)
+        decay = jnp.exp(last)
+        for group in range(groups_here):
+            cols = slice(group * group_width, (group + 1) * group_width)
+            b_here = bc_rows[rows, group * STATE : (group + 1) * STATE]
+            fresh = lax.dot_general(
+                b_here, weighted[:, cols], (((0,), (0,)), ((), ())), preferred_element_type=F32
+            )
+            state[:, cols] = old[:, cols] * decay[:, cols] + fresh
+        return total + last
+
+    total = lax.fori_loop(0, blocks, states_of, jnp.zeros((1, width), F32))
+    slot_f[sp] = state[...].astype(BF16)
+    slot_a[sp] = jnp.broadcast_to(jnp.exp(total), slot_a.shape[1:])
+
+    def state_copies(source, target):
+        return (
+            remote(
+                slot_f.at[source], slot_f.at[source], st_send.at[0, target],
+                st_recv.at[0, source], (target, tp),
+            ),
+            remote(
+                slot_a.at[source], slot_a.at[source], st_send.at[1, target],
+                st_recv.at[1, source], (target, tp),
+            ),
+        )
+
+    for target in range(1, n_sp):
+        @pl.when(target > sp)
+        def _():
+            for copy in state_copies(sp, target):
+                copy.start()
+
+    forward(2)
+
+    def outputs_of(block, carry):
+        rows = rows_of(block)
+        cum = heads_cum[rows, :]
+        cum_t = cum.T
+        wide = jnp.exp(cum_seg[rows, :])
+        x_here = scaled[rows, :].astype(BF16)
+        before = entering[block]
+        for group in range(groups_here):
+            cols = slice(group * group_width, (group + 1) * group_width)
+            b_here = bc_rows[rows, group * STATE : (group + 1) * STATE]
+            c_here = bc_rows[rows, half + group * STATE : half + (group + 1) * STATE]
+            scores = lax.dot_general(
+                c_here, b_here, (((1,), (1,)), ((), ())), preferred_element_type=F32
+            )
+            parts = []
+            for index in range(group * group_heads, (group + 1) * group_heads):
+                gap = cum[:, index : index + 1] - cum_t[index : index + 1, :]
+                within = jnp.where(causal, jnp.exp(jnp.where(causal, gap, 0.0)), 0.0)
+                parts.append(
+                    jnp.dot(
+                        (scores * within).astype(BF16),
+                        x_here[:, index * HEAD_DIM : (index + 1) * HEAD_DIM],
+                        preferred_element_type=F32,
+                    )
+                )
+            inner = jnp.concatenate(parts, axis=1)
+            carried = jnp.dot(c_here, before[:, cols], preferred_element_type=F32)
+            y_buf[rows, cols] = inner + carried * wide[:, cols]
+        return carry
+
+    lax.fori_loop(0, blocks, outputs_of, 0)
+    forward(3)
+    finish(2)
+    project(2)
+
+    for source in range(n_sp - 1):
+        @pl.when(source < sp)
+        def _():
+            for copy in state_copies(source, sp):
+                copy.wait_recv()
+
+    state[...] = jnp.zeros_like(state)
+
+    def combine(source, carry):
+        state[...] = state[...] * slot_a[source, 0:1, :] + slot_f[source].astype(F32)
+        return carry
+
+    lax.fori_loop(0, sp, combine, 0)
+
+    def gate_of(block, before):
+        rows = rows_of(block)
+        wide = cum_seg[rows, :]
+        decay = jnp.exp(before + wide)
+        gate = proj[pl.ds(pl.multiple_of(block * BLOCK + HALO, 16), BLOCK), :]
+        silu = gate / (1.0 + jnp.exp(-gate))
+        for group in range(groups_here):
+            cols = slice(group * group_width, (group + 1) * group_width)
+            c_here = bc_rows[rows, half + group * STATE : half + (group + 1) * STATE]
+            carried = jnp.dot(c_here, state[:, cols].astype(BF16), preferred_element_type=F32)
+            gated = (y_buf[rows, cols] + carried * decay[:, cols]) * silu[:, cols]
+            mixed[rows, cols] = (gated * inverse_rms(gated) * gain_ref[:, cols]).astype(BF16)
+        return before + wide[BLOCK - 1 : BLOCK, :]
+
+    lax.fori_loop(0, blocks, gate_of, jnp.zeros((1, width), F32))
+    finish(3)
+
+    partner = tp + 1 - 2 * lax.rem(tp, 2)
+    across = lax.rem(tp + 2, n_tp)
+    across_partner = lax.rem(partner + 2, n_tp)
+
+    def product(index):
+        rows = pl.ds(pl.multiple_of(index * share, 16), share)
+        return jnp.dot(mixed[rows, :], gath_o[...], preferred_element_type=F32).astype(BF16)
+
+    def pair_copy(slot, where):
+        return remote(
+            part.at[slot], pair_in.at[slot], rs_send.at[slot], rs_recv.at[slot], (sp, where)
+        )
+
+    part[0] = product(across_partner)
+    pair_copy(0, partner).start()
+    part[1] = product(partner)
+    pair_copy(1, partner).start()
+    mine = product(across)
+    pair_copy(0, partner).wait_recv()
+    part[2] = (mine.astype(F32) + pair_in[0].astype(F32)).astype(BF16)
+    pair_copy(2, across).start()
+    kept = product(tp).astype(F32)
+    pair_copy(1, partner).wait_recv()
+    kept = kept + pair_in[1].astype(F32)
+    pair_copy(2, across).wait_recv()
+    out_ref[...] = (kept + pair_in[2].astype(F32)).astype(BF16)
+
+    pair_copy(0, partner).wait_send()
+    pair_copy(1, partner).wait_send()
+    pair_copy(2, across).wait_send()
+    for chunk in range(4):
+        for step in range(n_z):
+            x_copy(chunk, step).wait_send()
+        for step in range(1, n_z):
+            z_copy(chunk, step).wait_send()
+    for target in range(1, n_sp):
+        @pl.when(target > sp)
+        def _():
+            for copy in state_copies(sp, target):
+                copy.wait_send()
+
+
+def fused_body(
+    tokens, in_gain, w_x, w_z, w_b, w_c, w_dt, conv_x, conv_b, conv_c, dt_bias, a_log, out_gain,
+    w_out,
+):
+    n_sp = lax.axis_size("sp")
+    n_tp = lax.axis_size("tp")
+    tp = lax.axis_index("tp")
+    share, features = tokens.shape
+    seg_rows = share * n_tp
+    blocks = seg_rows // BLOCK
+    width = w_x.shape[1]
+    width_b = w_b.shape[1]
+    heads_here = width // HEAD_DIM
+    lanes = 128
+
+    def cut(array, size, axis):
+        return lax.dynamic_slice_in_dim(array, tp * size, size, axis)
+
+    def wide_row(row):
+        return jnp.pad(row, (0, lanes - heads_here))[None]
+
+    w_bc = jnp.concatenate([w_b, w_c], axis=1)
+    taps_bc = jnp.concatenate([cut(conv_b, width_b, 1), cut(conv_c, width_b, 1)], axis=1)
+    dt_weight = jnp.pad(cut(w_dt, heads_here, 1), ((0, 0), (0, lanes - heads_here)))
+    args = (
+        tokens,
+        in_gain[None],
+        w_x,
+        w_bc,
+        w_z,
+        w_out,
+        dt_weight,
+        cut(conv_x, width, 1),
+        taps_bc,
+        wide_row(cut(dt_bias, heads_here, 0)),
+        wide_row(jnp.exp(cut(a_log, heads_here, 0))),
+        cut(out_gain, width, 0)[None],
+    )
+    dma = pltpu.SemaphoreType.DMA
+    vmem = pltpu.VMEM
+    n_z = n_sp // 2
+    return pl.pallas_call(
+        lambda *refs: mixer_kernel(n_sp, n_tp, *refs),
+        name="mixer",
+        out_shape=jax.ShapeDtypeStruct((share, features), BF16),
+        in_specs=[pl.BlockSpec(memory_space=vmem)] * len(args),
+        out_specs=pl.BlockSpec(memory_space=vmem),
+        scratch_shapes=[
+            vmem((seg_rows + HALO, features), BF16),
+            vmem((3, features, width), BF16),
+            vmem((width, features), BF16),
+            vmem((seg_rows + HALO, width), F32),
+            vmem((seg_rows, width), F32),
+            vmem((seg_rows, 2 * width_b), BF16),
+            vmem((seg_rows, lanes), F32),
+            vmem((seg_rows, width), F32),
+            vmem((seg_rows, lanes), F32),
+            vmem((blocks, STATE, width), BF16),
+            vmem((STATE, width), F32),
+            vmem((seg_rows, width), F32),
+            vmem((seg_rows, width), BF16),
+            vmem((3, share, features), BF16),
+            vmem((3, share, features), BF16),
+            vmem((n_sp, STATE, width), BF16),
+            vmem((n_sp, 8, width), F32),
+            dma((n_tp - 1,)),
+            dma((n_tp,)),
+            dma((n_tp,)),
+            dma((1,)),
+            dma((4, n_z)),
+            dma((4, n_z)),
+            dma((4, n_sp)),
+            dma((4,)),
+            dma((2, n_sp)),
+            dma((2, n_sp)),
+            dma((3,)),
+            dma((3,)),
+        ],
+        compiler_params=pltpu.CompilerParams(
+            has_side_effects=True, vmem_limit_bytes=60 * 1024 * 1024
+        ),
+    )(*args)
+
+
 def solution(mesh):
     in_specs = (
         P(("sp", "tp"), None),
@@ -216,4 +670,6 @@
         P("tp", "sp"),
     )
     out_specs = P(("sp", "tp"), None)
-    return jax.shard_map(body, mesh=mesh, in_specs=in_specs, out_specs=out_specs, check_vma=False)
+    fits = mesh.shape["tp"] == 4 and mesh.shape["sp"] in (2, 4, 6, 8)
+    plan = fused_body if fits else body
+    return jax.shard_map(plan, mesh=mesh, in_specs=in_specs, out_specs=out_specs, check_vma=False)

time: 368 us -> 167 us (0.45)
  waiting for transfers between devices: 246 us -> 0 us
  Pallas kernels: 0 us -> 155 us
  matrix products: 36 us -> 0 us
  local copies, waits for them, and re-layouts: 28.3 us -> 8.6 us
  blocking collectives: 15.2 us -> 0 us
  other arithmetic: 17 us -> 2.22 us
  between operations: 13.9 us -> 0.03 us
  starting transfers between devices: 7.66 us -> 0 us
    all_gather x7 -> x0, waiting for transfers between devices: 206 us -> none  [the longest x1 45.2 us: body(): lax.all_gather(w_x, 'sp', axis=0, tiled=True)]
    pallas_call x0 -> x1, Pallas kernels: none -> 155 us  [fused_body(): pl.pallas_call(lambda *refs: mixer_kernel(n_sp, n_tp, *refs), name='mixer...]
    dot_general x23 -> x0, matrix products: 36 us -> none  [the longest x4 13.6 us: fold_step(): return jnp.dot(gathered, rows_part, preferred_element_type=jnp.float32)]
    reduce_scatter x1 -> x0, waiting for transfers between devices: 34.7 us -> none  [body(): lax.psum_scatter(partial_sum.astype(jnp.bfloat16), 'tp', scatter_dimensio...]
    all_gather x1 -> x0, blocking collectives: 15.2 us -> none  [carried_in(): gathered = jax.tree.map(lambda a: lax.all_gather(a, axis), part)]
    reshape x5 -> x0, local copies, waits for them, and re-layouts: 8.94 us -> none  [the longest x2 5.8 us: body(): heads_out.reshape(seg_rows, width_x)]
    add x16 -> x0, other arithmetic: 7.39 us -> none  [the longest x6 6.37 us: chain(): earlier[1] * later[0][:, :, None, None] + later[1]]
    ppermute x3 -> x0, starting transfers between devices: 7.39 us -> none  [from_behind(): lax.ppermute(value, axis, [(source, source + steps) for source in range(f...]
  transfers between devices with their start and end apart: 11 -> 0, of which waited for: 9 -> 0; matrix products, arithmetic and copies ran while one was open for 20% -> 0% of each run, Pallas kernels for 0% -> 0%
where the time goes in v1:
time: 167 us; the launch traced here: 166 us
  Pallas kernels  155 us (93%)
  local copies, waits for them, and re-layouts  8.6 us (5%)
  other arithmetic  2.22 us (1%)
    pallas_call x1, Pallas kernels, fused_body(): pl.pallas_call(lambda *refs: mixer_kernel(n_sp, n_tp, *refs), name='mixer...  155 us
    dynamic_slice x5, local copies, waits for them, and re-layouts, cut(): return lax.dynamic_slice_in_dim(array, tp * size, size, axis)  4.1 us

profile of v1, /device:TPU:24, one launch (start us, length us, event | category | flops | bytes accessed | tf_op | source)
XLA Modules:
  0.0 166.2 jit_solution(18051078562126483104)
XLA Ops:
  0.0 0.0 copy-start
  0.0 0.0 copy-start.1
  0.0 0.8 dynamic_slice.25
  0.8 0.7 dynamic-slice_exponential_fusion
  1.5 0.6 pad_bitcast_fusion
  2.1 1.3 dynamic_slice.27
  3.5 1.3 constant_dynamic-slice_fusion.2.refs_7_
  4.7 0.7 constant_dynamic-slice_fusion
  5.4 0.6 pad_maximum_fusion.1.refs_8_
  6.0 0.0 copy-done
  6.0 0.0 copy-done.1
  6.1 1.6 pad_maximum_fusion.refs_3_
  7.7 0.3 copy.16
  8.0 0.9 pad.11.refs_6_
  8.9 155.4 %mixer.1 = bf16[160,2048]{1,0:T(8,128)(2,1)} custom-call(bf16[160,2048]{1,0:T(8,128)(2,1)} %refs_0_.1, f32[1,2048]{1,0:T(1,128)} %bitcast.6, bf16[256,512]{1,0:T(8,128)(2,1)} %refs_2_.1, bf16[256,512]{1,0:T(8,128)(2,1)} %pad_maximum_fusion.refs_3_, bf16[256,512]{1,0:T(8,128)(2,1)} %refs_4_.1, bf16[512,256]{1,0:T(8,128)(2,1)} %refs_5_.1, ...), custom_call_target="tpu_custom_call" | custom-call | tf_op jit(solution)/shard_map/mixer/pallas_call | solution.py:612
  164.3 2.0 %copy.18 = bf16[160,2048]{1,0:T(8,128)(2,1)} copy(bf16[160,2048]{1,0:T(8,128)(2,1)} %mixer.1) | data formatting | bytes 1310720
  (1 shorter events, 0.0 us)
Async XLA Ops:
  0.0 6.0 %copy-start = (bf16[2048,32]{0,1:T(8,128)(2,1)S(1)}, bf16[2048,32]{0,1:T(8,128)(2,1)}, u32[]{:S(2)}) copy-start(bf16[2048,32]{0,1:T(8,128)(2,1)} %param.20) | copy-start | bytes 393220
  0.0 6.0 %copy-start.1 = (bf16[256,256]{1,0:T(8,128)(2,1)S(1)}, bf16[256,256]{1,0:T(8,128)(2,1)}, u32[]{:S(2)}) copy-start(bf16[256,256]{1,0:T(8,128)(2,1)} %param.19) | copy-start | bytes 393220

commit v2 on v1

--- a/solution.py
+++ b/solution.py
@@ -212,15 +212,17 @@
     tok_ref,
     in_gain_ref,
     w_x_ref,
-    w_bc_ref,
     w_z_ref,
+    w_b_ref,
+    w_c_ref,
+    w_dt_ref,
+    conv_x_ref,
+    conv_b_ref,
+    conv_c_ref,
+    bias_ref,
+    a_log_ref,
+    gain_ref,
     w_o_ref,
-    w_dt_ref,
-    taps_x_ref,
-    taps_bc_ref,
-    bias_ref,
-    rate_ref,
-    gain_ref,
     out_ref,
     nall,
     gath,
@@ -235,10 +237,12 @@
     state,
     y_buf,
     mixed,
+    kept,
     part,
     pair_in,
     slot_f,
     slot_a,
+    slot_v,
     tok_send,
     tok_recv,
     halo_send,
@@ -249,6 +253,8 @@
     own_sem,
     st_send,
     st_recv,
+    cross_send,
+    cross_recv,
     rs_send,
     rs_recv,
 ):
@@ -265,8 +271,12 @@
     group_width = width // groups_here
     depth = w_x_ref.shape[0]
     n_z = n_sp // 2
-    beside = sp + 1 - 2 * lax.rem(sp, 2)
-    own_refs = (w_x_ref, w_bc_ref, w_z_ref, w_o_ref)
+    column = lax.rem(sp, 2)
+    plane = sp // 2
+    beside = sp + 1 - 2 * column
+    own_refs = (w_x_ref, w_b_ref, w_c_ref, w_z_ref, w_o_ref)
+    X, B, C, Z, O = range(5)
+    X_FIRST = (C,)
 
     def remote(src, dst, send, recv, where):
         return pltpu.make_async_remote_copy(
@@ -275,18 +285,112 @@
         )
 
     def place(chunk, source):
-        if chunk == 3:
+        if chunk == O:
             cols = w_o_ref.shape[1]
             return gath_o.at[:, pl.ds(pl.multiple_of(source * cols, cols), cols)]
-        return gath.at[chunk, pl.ds(pl.multiple_of(source * depth, depth), depth), :]
-
-    values = tok_ref[...].astype(F32)
-    normed = (values * inverse_rms(values) * in_gain_ref[...]).astype(BF16)
+        rows = pl.ds(pl.multiple_of(source * depth, depth), depth)
+        if chunk == X:
+            return gath.at[0, rows, :]
+        if chunk == Z:
+            return gath.at[2, rows, :]
+        return gath.at[1, rows, pl.ds(half * (chunk == C), half)]
+
+    upper = plane * 2 // n_z
+    mirrored = plane + upper * (n_z - 1 - 2 * plane)
+
+    def plane_at(turn):
+        if turn == 0:
+            return plane
+        near = turn - 1 + (turn + n_z - 1 - mirrored) // n_z
+        return near + upper * (n_z - 1 - 2 * near)
+
+    def x_copy(chunk, turn):
+        source = 2 * plane_at(turn) + column
+        src = own_refs[chunk] if turn == 0 else place(chunk, source)
+        return remote(
+            src, place(chunk, source), x_send.at[chunk, turn], w_recv.at[chunk, source],
+            (beside, tp),
+        )
+
+    def z_copy(chunk, other, turn, down):
+        side = 1 - column if other else column
+        source = 2 * plane_at(turn) + side
+        src = own_refs[chunk] if turn == 0 and not other else place(chunk, source)
+        target = sp - 2 if down else sp + 2
+        return remote(
+            src, place(chunk, source), z_send.at[chunk, other, turn, down],
+            w_recv.at[chunk, source], (target, tp),
+        )
+
+    def arrival(chunk, source):
+        return remote(
+            own_refs[chunk], place(chunk, source), x_send.at[chunk, 0], w_recv.at[chunk, source],
+            (beside, tp),
+        )
+
+    def own_copy(chunk):
+        return pltpu.make_async_copy(own_refs[chunk], place(chunk, sp), own_sem.at[chunk])
+
+    def along_z(chunk, other, turn, act):
+        if turn == 0:
+            goes_up = plane < n_z - 1
+            goes_down = plane > 0
+        else:
+            origin = plane_at(turn)
+            goes_up = jnp.logical_and(origin < plane, plane < n_z - 1)
+            goes_down = jnp.logical_and(origin > plane, plane > 0)
+
+        @pl.when(goes_up)
+        def _():
+            act(z_copy(chunk, other, turn, 0))
+
+        @pl.when(goes_down)
+        def _():
+            act(z_copy(chunk, other, turn, 1))
+
+    def start(copy):
+        copy.start()
+
+    def launch(chunk):
+        x_copy(chunk, 0).start()
+        along_z(chunk, 0, 0, start)
+        own_copy(chunk).start()
+
+    def pass_on(chunk, turn):
+        if chunk in X_FIRST:
+            for other in range(2):
+                if turn > 0 or other == 1:
+                    side = 1 - column if other else column
+                    arrival(chunk, 2 * plane_at(turn) + side).wait_recv()
+                    along_z(chunk, other, turn, start)
+        elif turn > 0:
+            arrival(chunk, 2 * plane_at(turn) + column).wait_recv()
+            along_z(chunk, 0, turn, start)
+            x_copy(chunk, turn).start()
+
+    def forward(chunk):
+        for turn in range(n_z):
+            pass_on(chunk, turn)
+
+    def finish_plane(chunk, turn):
+        if turn == 0:
+            own_copy(chunk).wait()
+        if chunk not in X_FIRST:
+            arrival(chunk, 2 * plane_at(turn) + 1 - column).wait_recv()
+
+    def finish(chunk):
+        for turn in range(n_z):
+            finish_plane(chunk, turn)
+
+    def drain(chunk):
+        for turn in range(n_z):
+            if chunk not in X_FIRST or turn == 0:
+                x_copy(chunk, turn).wait_send()
+            for other in range(1 + (chunk in X_FIRST)):
+                along_z(chunk, other, turn, lambda copy: copy.wait_send())
 
     def token_rows(index):
         return nall.at[pl.ds(pl.multiple_of(HALO + index * share, 16), share), :]
-
-    token_rows(tp)[...] = normed
 
     def token_copy(step):
         return remote(
@@ -300,55 +404,36 @@
             halo_recv.at[0], (lax.rem(sp + 1, n_sp), target),
         )
 
+    launch(X)
+    values = tok_ref[...].astype(F32)
+    token_rows(tp)[...] = (values * inverse_rms(values) * in_gain_ref[...]).astype(BF16)
+
+    lanes = log_step.shape[1]
+    head_of = lax.broadcasted_iota(jnp.int32, (w_dt_ref.shape[1], lanes), 0)
+    lane = lax.broadcasted_iota(jnp.int32, (w_dt_ref.shape[1], lanes), 1)
+    pick = jnp.logical_and(head_of == lane + tp * heads_here, lane < heads_here).astype(F32)
+    dt_weight = jnp.dot(
+        w_dt_ref[...], pick.astype(BF16), preferred_element_type=F32
+    ).astype(BF16)
+    bias = jnp.dot(bias_ref[...], pick, precision=HIGH, preferred_element_type=F32)
+    rate = jnp.dot(jnp.exp(a_log_ref[...]), pick, precision=HIGH, preferred_element_type=F32)
+    cols_x = pl.ds(pl.multiple_of(tp * width, width), width)
+    cols_b = pl.ds(pl.multiple_of(tp * half, half), half)
+    taps_x = conv_x_ref[:, cols_x]
+    taps_bc = jnp.concatenate([conv_b_ref[:, cols_b], conv_c_ref[:, cols_b]], axis=1)
+    gain = gain_ref[:, cols_x]
+
     @pl.when(tp == n_tp - 1)
     def _():
         for target in range(n_tp):
             halo_copy(target).start()
 
-    def z_copy(chunk, step):
-        return remote(
-            own_refs[chunk], place(chunk, sp), z_send.at[chunk, step], w_recv.at[chunk, sp],
-            (lax.rem(sp + 2 * step, n_sp), tp),
-        )
-
-    def x_copy(chunk, step):
-        source = lax.rem(sp + n_sp - 2 * step, n_sp)
-        src = own_refs[chunk] if step == 0 else place(chunk, source)
-        return remote(
-            src, place(chunk, source), x_send.at[chunk, step], w_recv.at[chunk, source],
-            (beside, tp),
-        )
-
-    def arrival(chunk, source):
-        return remote(
-            own_refs[chunk], place(chunk, source), z_send.at[chunk, 0], w_recv.at[chunk, source],
-            (beside, tp),
-        )
-
-    def own_copy(chunk):
-        return pltpu.make_async_copy(own_refs[chunk], place(chunk, sp), own_sem.at[chunk])
-
-    for chunk in range(4):
-        x_copy(chunk, 0).start()
-        for step in range(1, n_z):
-            z_copy(chunk, step).start()
-        if chunk == 0:
-            for step in range(1, n_tp):
-                token_copy(step).start()
-        own_copy(chunk).start()
-
-    def forward(chunk):
-        for step in range(1, n_z):
-            source = lax.rem(sp + n_sp - 2 * step, n_sp)
-            arrival(chunk, source).wait_recv()
-            x_copy(chunk, step).start()
-
-    def finish(chunk):
-        own_copy(chunk).wait()
-        for step in range(n_z):
-            arrival(chunk, lax.rem(beside + n_sp - 2 * step, n_sp)).wait_recv()
-
-    forward(0)
+    for step in range(1, n_tp):
+        token_copy(step).start()
+    launch(B)
+    launch(C)
+    launch(Z)
+    forward(X)
     for step in range(1, n_tp):
         source = lax.rem(tp + n_tp - step, n_tp)
         remote(
@@ -369,10 +454,9 @@
     def _():
         nall[pl.ds(0, HALO), :] = jnp.zeros((HALO, nall.shape[1]), BF16)
 
-    raw = jnp.dot(nall[pl.ds(HALO, seg_rows), :], w_dt_ref[...], preferred_element_type=F32)
-    raw = raw + bias_ref[...]
+    raw = jnp.dot(nall[pl.ds(HALO, seg_rows), :], dt_weight, preferred_element_type=F32)
+    raw = raw + bias
     log_step[...] = jnp.maximum(raw, 0.0) + jnp.log1p(jnp.exp(-jnp.abs(raw)))
-    lanes = log_step.shape[1]
     spread = (
         lax.broadcasted_iota(jnp.int32, (lanes, width), 0)
         == lax.broadcasted_iota(jnp.int32, (lanes, width), 1) // HEAD_DIM
@@ -381,33 +465,37 @@
         jnp.int32, (BLOCK, BLOCK), 1
     )
 
-    def project(chunk):
-        proj[...] = (
-            jnp.dot(nall[...], gath[chunk], preferred_element_type=F32).astype(BF16).astype(F32)
-        )
-
-    def conv(block, taps):
-        summed = jnp.zeros((BLOCK, width), F32)
-        start = block * BLOCK + HALO - (CONV - 1)
+    def project(weights, cols):
+        proj[:, cols] = (
+            jnp.dot(nall[...], weights, preferred_element_type=F32).astype(BF16).astype(F32)
+        )
+
+    def conv(block, taps, cols):
+        summed = jnp.zeros((BLOCK, taps.shape[1]), F32)
+        first = block * BLOCK + HALO - (CONV - 1)
         for offset in range(CONV):
             summed = summed + taps[offset : offset + 1, :] * proj[
-                start + offset : start + offset + BLOCK, :
+                first + offset : first + offset + BLOCK, cols
             ]
         return summed / (1.0 + jnp.exp(-summed))
 
-    forward(1)
-    finish(0)
-    project(0)
+    forward(B)
+    finish(X)
+    project(gath[0], slice(0, width))
     for block in range(blocks):
         rows = pl.ds(block * BLOCK, BLOCK)
         step_here = jnp.dot(log_step[rows, :], spread, precision=HIGH, preferred_element_type=F32)
-        scaled[rows, :] = conv(block, taps_x_ref[...]) * step_here
-
-    finish(1)
-    project(1)
-    for block in range(blocks):
-        rows = pl.ds(block * BLOCK, BLOCK)
-        bc_rows[rows, :] = conv(block, taps_bc_ref[...]).astype(BF16)
+        scaled[rows, :] = conv(block, taps_x, slice(0, width)) * step_here
+
+    def group_rows(cols):
+        project(gath[1, :, cols], cols)
+        for block in range(blocks):
+            rows = pl.ds(block * BLOCK, BLOCK)
+            bc_rows[rows, cols] = conv(block, taps_bc[:, cols], cols).astype(BF16)
+
+    pass_on(C, 0)
+    finish(B)
+    group_rows(slice(0, half))
 
     def rows_of(block):
         return pl.ds(pl.multiple_of(block * BLOCK, BLOCK), BLOCK)
@@ -417,7 +505,7 @@
 
     def states_of(block, total):
         rows = rows_of(block)
-        log_rate = -log_step[rows, :] * rate_ref[...]
+        log_rate = -log_step[rows, :] * rate
         cum = jnp.dot(tri, log_rate, precision=HIGH, preferred_element_type=F32)
         heads_cum[rows, :] = cum
         wide = jnp.dot(cum, spread, precision=HIGH, preferred_element_type=F32)
@@ -434,31 +522,41 @@
                 b_here, weighted[:, cols], (((0,), (0,)), ((), ())), preferred_element_type=F32
             )
             state[:, cols] = old[:, cols] * decay[:, cols] + fresh
-        return total + last
-
-    total = lax.fori_loop(0, blocks, states_of, jnp.zeros((1, width), F32))
-    slot_f[sp] = state[...].astype(BF16)
+        return total + cum[BLOCK - 1 : BLOCK, :]
+
+    total = lax.fori_loop(0, blocks, states_of, jnp.zeros((1, lanes), F32))
+    slot_f[plane] = state[...].astype(BF16)
     slot_a[sp] = jnp.broadcast_to(jnp.exp(total), slot_a.shape[1:])
 
-    def state_copies(source, target):
-        return (
-            remote(
-                slot_f.at[source], slot_f.at[source], st_send.at[0, target],
-                st_recv.at[0, source], (target, tp),
-            ),
-            remote(
-                slot_a.at[source], slot_a.at[source], st_send.at[1, target],
-                st_recv.at[1, source], (target, tp),
-            ),
-        )
-
-    for target in range(1, n_sp):
-        @pl.when(target > sp)
-        def _():
-            for copy in state_copies(sp, target):
-                copy.start()
-
-    forward(2)
+    def state_copy(source_plane, target_plane):
+        return remote(
+            slot_f.at[source_plane], slot_f.at[source_plane], st_send.at[0, target_plane],
+            st_recv.at[0, source_plane], (2 * target_plane + column, tp),
+        )
+
+    def decay_copy(source, target):
+        return remote(
+            slot_a.at[source], slot_a.at[source], st_send.at[1, target], st_recv.at[1, source],
+            (target, tp),
+        )
+
+    def to_later(act):
+        for target in range(1, n_sp):
+            @pl.when(target > sp)
+            def _():
+                act(decay_copy(sp, target))
+
+        for target in range(1, n_z):
+            @pl.when(target > plane)
+            def _():
+                act(state_copy(plane, target))
+
+    to_later(start)
+    launch(O)
+    for turn in range(1, n_z):
+        pass_on(C, turn)
+    finish(C)
+    group_rows(slice(half, width))
 
     def outputs_of(block, carry):
         rows = rows_of(block)
@@ -491,23 +589,55 @@
         return carry
 
     lax.fori_loop(0, blocks, outputs_of, 0)
-    forward(3)
-    finish(2)
-    project(2)
+    forward(Z)
+
+    def decay_of(index):
+        return jnp.dot(slot_a[index], spread, precision=HIGH, preferred_element_type=F32)[0:1]
 
     for source in range(n_sp - 1):
         @pl.when(source < sp)
         def _():
-            for copy in state_copies(source, sp):
-                copy.wait_recv()
+            decay_copy(source, sp).wait_recv()
 
     state[...] = jnp.zeros_like(state)
-
-    def combine(source, carry):
-        state[...] = state[...] * slot_a[source, 0:1, :] + slot_f[source].astype(F32)
-        return carry
-
-    lax.fori_loop(0, sp, combine, 0)
+    for below in range(n_z - 1):
+        @pl.when(below < plane)
+        def _():
+            state_copy(below, plane).wait_recv()
+            after = decay_of(2 * below + 1)
+            lead = decay_of(2 * below) * after
+            fresh = slot_f[below].astype(F32)
+
+            @pl.when(column == 0)
+            def _():
+                state[...] = state[...] * lead + fresh * after
+
+            @pl.when(column == 1)
+            def _():
+                state[...] = state[...] * lead + fresh
+
+    @pl.when(column == 0)
+    def _():
+        slot_v[0] = (state[...] * decay_of(sp) + slot_f[plane].astype(F32)).astype(BF16)
+
+    @pl.when(column == 1)
+    def _():
+        slot_v[0] = state[...].astype(BF16)
+
+    cross = remote(slot_v.at[0], slot_v.at[1], cross_send.at[0], cross_recv.at[0], (beside, tp))
+    cross.start()
+    finish(Z)
+    project(gath[2], slice(0, width))
+    pass_on(O, 1)
+    cross.wait_recv()
+
+    @pl.when(column == 0)
+    def _():
+        state[...] = state[...] + slot_v[1].astype(F32)
+
+    @pl.when(column == 1)
+    def _():
+        state[...] = state[...] * decay_of(sp - 1) + slot_v[1].astype(F32)
 
     def gate_of(block, before):
         rows = rows_of(block)
@@ -520,52 +650,63 @@
             c_here = bc_rows[rows, half + group * STATE : half + (group + 1) * STATE]
             carried = jnp.dot(c_here, state[:, cols].astype(BF16), preferred_element_type=F32)
             gated = (y_buf[rows, cols] + carried * decay[:, cols]) * silu[:, cols]
-            mixed[rows, cols] = (gated * inverse_rms(gated) * gain_ref[:, cols]).astype(BF16)
+            mixed[rows, cols] = (gated * inverse_rms(gated) * gain[:, cols]).astype(BF16)
         return before + wide[BLOCK - 1 : BLOCK, :]
 
     lax.fori_loop(0, blocks, gate_of, jnp.zeros((1, width), F32))
-    finish(3)
 
     partner = tp + 1 - 2 * lax.rem(tp, 2)
     across = lax.rem(tp + 2, n_tp)
     across_partner = lax.rem(partner + 2, n_tp)
-
-    def product(index):
-        rows = pl.ds(pl.multiple_of(index * share, 16), share)
-        return jnp.dot(mixed[rows, :], gath_o[...], preferred_element_type=F32).astype(BF16)
-
-    def pair_copy(slot, where):
+    span = 2 * w_o_ref.shape[1]
+
+    def pair_copy(kind, turn, where):
         return remote(
-            part.at[slot], pair_in.at[slot], rs_send.at[slot], rs_recv.at[slot], (sp, where)
-        )
-
-    part[0] = product(across_partner)
-    pair_copy(0, partner).start()
-    part[1] = product(partner)
-    pair_copy(1, partner).start()
-    mine = product(across)
-    pair_copy(0, partner).wait_recv()
-    part[2] = (mine.astype(F32) + pair_in[0].astype(F32)).astype(BF16)
-    pair_copy(2, across).start()
-    kept = product(tp).astype(F32)
-    pair_copy(1, partner).wait_recv()
-    kept = kept + pair_in[1].astype(F32)
-    pair_copy(2, across).wait_recv()
-    out_ref[...] = (kept + pair_in[2].astype(F32)).astype(BF16)
-
-    pair_copy(0, partner).wait_send()
-    pair_copy(1, partner).wait_send()
-    pair_copy(2, across).wait_send()
-    for chunk in range(4):
-        for step in range(n_z):
-            x_copy(chunk, step).wait_send()
-        for step in range(1, n_z):
-            z_copy(chunk, step).wait_send()
-    for target in range(1, n_sp):
-        @pl.when(target > sp)
-        def _():
-            for copy in state_copies(sp, target):
-                copy.wait_send()
+            part.at[kind, turn], pair_in.at[kind, turn], rs_send.at[kind, turn],
+            rs_recv.at[kind, turn], (sp, where),
+        )
+
+    def columns_at(turn):
+        return pl.ds(pl.multiple_of(plane_at(turn) * span, span), span)
+
+    for turn in range(n_z):
+        if 0 < turn < n_z - 1:
+            pass_on(O, turn + 1)
+        finish_plane(O, turn)
+        weights = gath_o[:, columns_at(turn)]
+
+        def product(index):
+            rows = pl.ds(pl.multiple_of(index * share, 16), share)
+            return (
+                jnp.dot(mixed[rows, :], weights, preferred_element_type=F32)
+                .astype(BF16)
+                .astype(F32)
+            )
+
+        part[0, turn] = product(across_partner).astype(BF16)
+        pair_copy(0, turn, partner).start()
+        part[1, turn] = product(partner).astype(BF16)
+        pair_copy(1, turn, partner).start()
+        mine = product(across)
+        kept[turn] = product(tp)
+        pair_copy(0, turn, partner).wait_recv()
+        part[2, turn] = (mine + pair_in[0, turn].astype(F32)).astype(BF16)
+        pair_copy(2, turn, across).start()
+
+    for turn in range(n_z):
+        pair_copy(1, turn, partner).wait_recv()
+        pair_copy(2, turn, across).wait_recv()
+        whole = kept[turn] + pair_in[1, turn].astype(F32) + pair_in[2, turn].astype(F32)
+        out_ref[:, columns_at(turn)] = whole.astype(BF16)
+
+    for turn in range(n_z):
+        pair_copy(0, turn, partner).wait_send()
+        pair_copy(1, turn, partner).wait_send()
+        pair_copy(2, turn, across).wait_send()
+    for chunk in range(5):
+        drain(chunk)
+    to_later(lambda copy: copy.wait_send())
+    cross.wait_send()
 
 
 def fused_body(
@@ -574,41 +715,20 @@
 ):
     n_sp = lax.axis_size("sp")
     n_tp = lax.axis_size("tp")
-    tp = lax.axis_index("tp")
+    n_z = n_sp // 2
     share, features = tokens.shape
     seg_rows = share * n_tp
     blocks = seg_rows // BLOCK
     width = w_x.shape[1]
     width_b = w_b.shape[1]
-    heads_here = width // HEAD_DIM
     lanes = 128
-
-    def cut(array, size, axis):
-        return lax.dynamic_slice_in_dim(array, tp * size, size, axis)
-
-    def wide_row(row):
-        return jnp.pad(row, (0, lanes - heads_here))[None]
-
-    w_bc = jnp.concatenate([w_b, w_c], axis=1)
-    taps_bc = jnp.concatenate([cut(conv_b, width_b, 1), cut(conv_c, width_b, 1)], axis=1)
-    dt_weight = jnp.pad(cut(w_dt, heads_here, 1), ((0, 0), (0, lanes - heads_here)))
+    span = features // n_z
     args = (
-        tokens,
-        in_gain[None],
-        w_x,
-        w_bc,
-        w_z,
-        w_out,
-        dt_weight,
-        cut(conv_x, width, 1),
-        taps_bc,
-        wide_row(cut(dt_bias, heads_here, 0)),
-        wide_row(jnp.exp(cut(a_log, heads_here, 0))),
-        cut(out_gain, width, 0)[None],
+        tokens, in_gain[None], w_x, w_z, w_b, w_c, w_dt, conv_x, conv_b, conv_c, dt_bias[None],
+        a_log[None], out_gain[None], w_out,
     )
     dma = pltpu.SemaphoreType.DMA
     vmem = pltpu.VMEM
-    n_z = n_sp // 2
     return pl.pallas_call(
         lambda *refs: mixer_kernel(n_sp, n_tp, *refs),
         name="mixer",
@@ -629,22 +749,26 @@
             vmem((STATE, width), F32),
             vmem((seg_rows, width), F32),
             vmem((seg_rows, width), BF16),
-            vmem((3, share, features), BF16),
-            vmem((3, share, features), BF16),
-            vmem((n_sp, STATE, width), BF16),
-            vmem((n_sp, 8, width), F32),
+            vmem((n_z, share, span), F32),
+            vmem((3, n_z, share, span), BF16),
+            vmem((3, n_z, share, span), BF16),
+            vmem((n_z, STATE, width), BF16),
+            vmem((n_sp, 8, lanes), F32),
+            vmem((2, STATE, width), BF16),
             dma((n_tp - 1,)),
             dma((n_tp,)),
             dma((n_tp,)),
             dma((1,)),
-            dma((4, n_z)),
-            dma((4, n_z)),
-            dma((4, n_sp)),
-            dma((4,)),
+            dma((5, 2, n_z, 2)),
+            dma((5, n_z)),
+            dma((5, n_sp)),
+            dma((5,)),
             dma((2, n_sp)),
             dma((2, n_sp)),
-            dma((3,)),
-            dma((3,)),
+            dma((1,)),
+            dma((1,)),
+            dma((3, n_z)),
+            dma((3, n_z)),
         ],
         compiler_params=pltpu.CompilerParams(
             has_side_effects=True, vmem_limit_bytes=60 * 1024 * 1024
@@ -670,6 +794,6 @@
         P("tp", "sp"),
     )
     out_specs = P(("sp", "tp"), None)
-    fits = mesh.shape["tp"] == 4 and mesh.shape["sp"] in (2, 4, 6, 8)
+    fits = mesh.shape["tp"] == 4 and mesh.shape["sp"] in (4, 6, 8)
     plan = fused_body if fits else body
     return jax.shard_map(plan, mesh=mesh, in_specs=in_specs, out_specs=out_specs, check_vma=False)

time: 167 us -> 149 us (0.89)
  Pallas kernels: 155 us -> 144 us
  local copies, waits for them, and re-layouts: 8.6 us -> 3.89 us
  other arithmetic: 2.22 us -> 0 us
    pallas_call x1, Pallas kernels: 155 us -> 144 us  [fused_body(): pl.pallas_call(lambda *refs: mixer_kernel(n_sp, n_tp, *refs), name='mixer...]
    dynamic_slice x5 -> x0, local copies, waits for them, and re-layouts: 4.1 us -> none  [cut(): return lax.dynamic_slice_in_dim(array, tp * size, size, axis)]
    concatenate x2 -> x0, other arithmetic: 2.22 us -> none  [the longest x1 1.62 us: fused_body(): w_bc = jnp.concatenate([w_b, w_c], axis=1)]
    unnamed x6 -> x2, local copies, waits for them, and re-layouts: 2.26 us -> 3.89 us
where the time goes in v2:
time: 149 us; the launch traced here: 148 us
  Pallas kernels  144 us (97%)
  local copies, waits for them, and re-layouts  3.89 us (3%)
    pallas_call x1, Pallas kernels, fused_body(): pl.pallas_call(lambda *refs: mixer_kernel(n_sp, n_tp, *refs), name='mixer...  144 us
    unnamed x2, local copies, waits for them, and re-layouts  3.89 us

profile of v2, /device:TPU:24, one launch (start us, length us, event | category | flops | bytes accessed | tf_op | source)
XLA Modules:
  0.0 148.1 jit_solution(8514300116234465255)
XLA Ops:
  0.0 1.9 %copy.15.refs_6_ = bf16[2048,32]{1,0:T(8,128)(2,1)} copy(bf16[2048,32]{0,1:T(8,128)(2,1)} %param.20) | data formatting | bytes 262144 | tf_op args[6]
  1.9 144.2 %mixer.1 = bf16[160,2048]{1,0:T(8,128)(2,1)} custom-call(bf16[160,2048]{1,0:T(8,128)(2,1)} %refs_0_.1, f32[1,2048]{1,0:T(1,128)} %bitcast.4, bf16[256,512]{1,0:T(8,128)(2,1)} %refs_2_.1, bf16[256,512]{1,0:T(8,128)(2,1)} %refs_3_.1, bf16[256,256]{1,0:T(8,128)(2,1)} %refs_4_.1, bf16[256,256]{1,0:T(8,128)(2,1)} %refs_5_.1, bf16[2048,32]{1,0:T(8,128)(2,1)} %copy.15.refs_6_, ...), custom_call_target="tpu_custom_call" | custom-call | tf_op jit(solution)/shard_map/mixer/pallas_call | solution.py:732
  146.1 2.0 %copy.17 = bf16[160,2048]{1,0:T(8,128)(2,1)} copy(bf16[160,2048]{1,0:T(8,128)(2,1)} %mixer.1) | data formatting | bytes 1310720

commit v3 on v2

--- a/solution.py
+++ b/solution.py
@@ -312,15 +312,24 @@
             (beside, tp),
         )
 
-    def z_copy(chunk, other, turn, down):
-        side = 1 - column if other else column
-        source = 2 * plane_at(turn) + side
-        src = own_refs[chunk] if turn == 0 and not other else place(chunk, source)
-        target = sp - 2 if down else sp + 2
+    def z_copy(chunk, other, turn):
+        source = 2 * plane + (1 - column if other else column)
+        src = place(chunk, source) if other else own_refs[chunk]
         return remote(
-            src, place(chunk, source), z_send.at[chunk, other, turn, down],
-            w_recv.at[chunk, source], (target, tp),
-        )
+            src, place(chunk, source), z_send.at[chunk, other, turn], w_recv.at[chunk, source],
+            (2 * plane_at(turn) + column, tp),
+        )
+
+    def relay(chunk):
+        origin = plane_at(n_z - 1)
+        source = 2 * origin + column
+        return remote(
+            place(chunk, source), place(chunk, source), z_send.at[chunk, 0, 0],
+            w_recv.at[chunk, source], (2 * (n_z - 1 - origin) + column, tp),
+        )
+
+    relayed = n_z == 4
+    inside = jnp.logical_and(plane > 0, plane < n_z - 1)
 
     def arrival(chunk, source):
         return remote(
@@ -331,63 +340,63 @@
     def own_copy(chunk):
         return pltpu.make_async_copy(own_refs[chunk], place(chunk, sp), own_sem.at[chunk])
 
-    def along_z(chunk, other, turn, act):
-        if turn == 0:
-            goes_up = plane < n_z - 1
-            goes_down = plane > 0
-        else:
-            origin = plane_at(turn)
-            goes_up = jnp.logical_and(origin < plane, plane < n_z - 1)
-            goes_down = jnp.logical_and(origin > plane, plane > 0)
-
-        @pl.when(goes_up)
-        def _():
-            act(z_copy(chunk, other, turn, 0))
-
-        @pl.when(goes_down)
-        def _():
-            act(z_copy(chunk, other, turn, 1))
-
     def start(copy):
         copy.start()
 
+    def wait_send(copy):
+        copy.wait_send()
+
+    def along_z(chunk, other, act):
+        for turn in range(1, n_z):
+            if relayed and turn == n_z - 1 and chunk not in X_FIRST:
+                @pl.when(inside)
+                def _():
+                    act(z_copy(chunk, other, turn))
+            else:
+                act(z_copy(chunk, other, turn))
+
     def launch(chunk):
         x_copy(chunk, 0).start()
-        along_z(chunk, 0, 0, start)
+        along_z(chunk, 0, start)
         own_copy(chunk).start()
 
+    def cross_over(chunk):
+        arrival(chunk, beside).wait_recv()
+        along_z(chunk, 1, start)
+
     def pass_on(chunk, turn):
-        if chunk in X_FIRST:
-            for other in range(2):
-                if turn > 0 or other == 1:
-                    side = 1 - column if other else column
-                    arrival(chunk, 2 * plane_at(turn) + side).wait_recv()
-                    along_z(chunk, other, turn, start)
-        elif turn > 0:
-            arrival(chunk, 2 * plane_at(turn) + column).wait_recv()
-            along_z(chunk, 0, turn, start)
-            x_copy(chunk, turn).start()
-
-    def forward(chunk):
-        for turn in range(n_z):
-            pass_on(chunk, turn)
+        arrival(chunk, 2 * plane_at(turn) + column).wait_recv()
+        if relayed and turn == n_z - 1:
+            @pl.when(inside)
+            def _():
+                relay(chunk).start()
+        x_copy(chunk, turn).start()
 
     def finish_plane(chunk, turn):
         if turn == 0:
             own_copy(chunk).wait()
         if chunk not in X_FIRST:
             arrival(chunk, 2 * plane_at(turn) + 1 - column).wait_recv()
+        elif turn > 0:
+            for side in range(2):
+                arrival(chunk, 2 * plane_at(turn) + side).wait_recv()
 
     def finish(chunk):
         for turn in range(n_z):
             finish_plane(chunk, turn)
 
     def drain(chunk):
-        for turn in range(n_z):
-            if chunk not in X_FIRST or turn == 0:
-                x_copy(chunk, turn).wait_send()
-            for other in range(1 + (chunk in X_FIRST)):
-                along_z(chunk, other, turn, lambda copy: copy.wait_send())
+        along_z(chunk, 0, wait_send)
+        x_copy(chunk, 0).wait_send()
+        if chunk in X_FIRST:
+            along_z(chunk, 1, wait_send)
+            return
+        for turn in range(1, n_z):
+            x_copy(chunk, turn).wait_send()
+        if relayed:
+            @pl.when(inside)
+            def _():
+                relay(chunk).wait_send()
 
     def token_rows(index):
         return nall.at[pl.ds(pl.multiple_of(HALO + index * share, 16), share), :]
@@ -409,11 +418,16 @@
     token_rows(tp)[...] = (values * inverse_rms(values) * in_gain_ref[...]).astype(BF16)
 
     lanes = log_step.shape[1]
-    head_of = lax.broadcasted_iota(jnp.int32, (w_dt_ref.shape[1], lanes), 0)
-    lane = lax.broadcasted_iota(jnp.int32, (w_dt_ref.shape[1], lanes), 1)
-    pick = jnp.logical_and(head_of == lane + tp * heads_here, lane < heads_here).astype(F32)
+    heads_all = w_dt_ref.shape[0]
+
+    def picked(shape, head_axis):
+        head = lax.broadcasted_iota(jnp.int32, shape, head_axis)
+        lane = lax.broadcasted_iota(jnp.int32, shape, 1 - head_axis)
+        return jnp.logical_and(head == lane + tp * heads_here, lane < heads_here).astype(F32)
+
+    pick = picked((heads_all, lanes), 0)
     dt_weight = jnp.dot(
-        w_dt_ref[...], pick.astype(BF16), preferred_element_type=F32
+        picked((lanes, heads_all), 1).astype(BF16), w_dt_ref[...], preferred_element_type=F32
     ).astype(BF16)
     bias = jnp.dot(bias_ref[...], pick, precision=HIGH, preferred_element_type=F32)
     rate = jnp.dot(jnp.exp(a_log_ref[...]), pick, precision=HIGH, preferred_element_type=F32)
@@ -432,8 +446,14 @@
         token_copy(step).start()
     launch(B)
     launch(C)
+
+    def forward(chunk):
+        for turn in range(1, n_z):
+            pass_on(chunk, turn)
+
+    forward(X)
+    cross_over(C)
     launch(Z)
-    forward(X)
     for step in range(1, n_tp):
         source = lax.rem(tp + n_tp - step, n_tp)
         remote(
@@ -454,7 +474,10 @@
     def _():
         nall[pl.ds(0, HALO), :] = jnp.zeros((HALO, nall.shape[1]), BF16)
 
-    raw = jnp.dot(nall[pl.ds(HALO, seg_rows), :], dt_weight, preferred_element_type=F32)
+    raw = lax.dot_general(
+        nall[pl.ds(HALO, seg_rows), :], dt_weight, (((1,), (1,)), ((), ())),
+        preferred_element_type=F32,
+    )
     raw = raw + bias
     log_step[...] = jnp.maximum(raw, 0.0) + jnp.log1p(jnp.exp(-jnp.abs(raw)))
     spread = (
@@ -493,7 +516,8 @@
             rows = pl.ds(block * BLOCK, BLOCK)
             bc_rows[rows, cols] = conv(block, taps_bc[:, cols], cols).astype(BF16)
 
-    pass_on(C, 0)
+    for turn in range(1, n_z - 1):
+        pass_on(Z, turn)
     finish(B)
     group_rows(slice(0, half))
 
@@ -553,8 +577,7 @@
 
     to_later(start)
     launch(O)
-    for turn in range(1, n_z):
-        pass_on(C, turn)
+    pass_on(Z, n_z - 1)
     finish(C)
     group_rows(slice(half, width))
 
@@ -589,7 +612,7 @@
         return carry
 
     lax.fori_loop(0, blocks, outputs_of, 0)
-    forward(Z)
+    pass_on(O, 1)
 
     def decay_of(index):
         return jnp.dot(slot_a[index], spread, precision=HIGH, preferred_element_type=F32)[0:1]
@@ -628,7 +651,6 @@
     cross.start()
     finish(Z)
     project(gath[2], slice(0, width))
-    pass_on(O, 1)
     cross.wait_recv()
 
     @pl.when(column == 0)
@@ -724,7 +746,7 @@
     lanes = 128
     span = features // n_z
     args = (
-        tokens, in_gain[None], w_x, w_z, w_b, w_c, w_dt, conv_x, conv_b, conv_c, dt_bias[None],
+        tokens, in_gain[None], w_x, w_z, w_b, w_c, w_dt.T, conv_x, conv_b, conv_c, dt_bias[None],
         a_log[None], out_gain[None], w_out,
     )
     dma = pltpu.SemaphoreType.DMA
@@ -759,7 +781,7 @@
             dma((n_tp,)),
             dma((n_tp,)),
             dma((1,)),
-            dma((5, 2, n_z, 2)),
+            dma((5, 2, n_z)),
             dma((5, n_z)),
             dma((5, n_sp)),
             dma((5,)),

time: 149 us -> 141 us (0.946)
  Pallas kernels: 144 us -> 139 us
  local copies, waits for them, and re-layouts: 3.89 us -> 1.98 us
    pallas_call x1, Pallas kernels: 144 us -> 139 us  [fused_body(): pl.pallas_call(lambda *refs: mixer_kernel(n_sp, n_tp, *refs), name='mixer...]
    unnamed x2 -> x1, local copies, waits for them, and re-layouts: 3.89 us -> 1.98 us
where the time goes in v3:
time: 141 us
  Pallas kernels  139 us (99%)
  local copies, waits for them, and re-layouts  1.98 us (1%)
    pallas_call x1, Pallas kernels, fused_body(): pl.pallas_call(lambda *refs: mixer_kernel(n_sp, n_tp, *refs), name='mixer...  139 us

profile of v3, /device:TPU:24, one launch (start us, length us, event | category | flops | bytes accessed | tf_op | source)
XLA Modules:
  0.0 140.8 jit_solution(74744566955790557)
XLA Ops:
  0.0 138.8 %mixer.1 = bf16[160,2048]{1,0:T(8,128)(2,1)} custom-call(bf16[160,2048]{1,0:T(8,128)(2,1)} %refs_0_.1, f32[1,2048]{1,0:T(1,128)} %bitcast.6, bf16[256,512]{1,0:T(8,128)(2,1)} %refs_2_.1, bf16[256,512]{1,0:T(8,128)(2,1)} %refs_3_.1, bf16[256,256]{1,0:T(8,128)(2,1)} %refs_4_.1, bf16[256,256]{1,0:T(8,128)(2,1)} %refs_5_.1, bf16[32,2048]{1,0:T(8,128)(2,1)} %bitcast.5, ...), custom_call_target="tpu_custom_call" | custom-call | tf_op jit(solution)/shard_map/mixer/pallas_call | solution.py:754
  138.8 2.0 %copy.16 = bf16[160,2048]{1,0:T(8,128)(2,1)} copy(bf16[160,2048]{1,0:T(8,128)(2,1)} %mixer.1) | data formatting | bytes 1310720
